TPU v7x, 32 devices: a whole 2x2x4 slice. The times are simulated.
32 devices in a mesh: ep: 8 (over z, y), tp: 4 (over x, core).
Axes of the slice: x: 2, y: 2, z: 4, core: 2. Of those that a mesh axis runs over, the one named last changes fastest.
Arguments:
- query_rows: bfloat16 [3072, 1024], P('ep', 'tp'), may hold values from -6 to 6
- key_rows: bfloat16 [3072, 512], P('ep', 'tp'), may hold values from -6 to 6
- value_rows: bfloat16 [3072, 512], P('ep', 'tp'), may hold values from -6 to 6
- break_bias: bfloat16 [3072, 16], P('ep', 'tp'), may hold values from -14 to 0
- mixer_weight: bfloat16 [1024, 2048], P('tp'), may hold values from -0.1875 to 0.1875
- mixer_gain: bfloat16 [2048], replicated, may hold values from 0.099609375 to 1.8984375
- expert_input: bfloat16 [4096, 2048], P(('ep', 'tp')), may hold values from -6 to 6
- expert_gain: bfloat16 [2048], replicated, may hold values from 0.099609375 to 1.8984375
- route_ids: int32 [4096, 2], P('ep'), may hold values from 0 to 15, all different within a row; in each aligned block of 128 rows (0 to 127, 128 to 255, ...) at most 32 rows name the same one
- route_weights: float32 [4096, 2], P(('ep', 'tp')), may hold values from 0.2 to 2
- expert_gate: bfloat16 [16, 2048, 2048], P('ep', None, 'tp'), may hold values from -0.125 to 0.125
- expert_up: bfloat16 [16, 2048, 2048], P('ep', None, 'tp'), may hold values from -0.125 to 0.125
- expert_down: bfloat16 [16, 2048, 2048], P('ep', 'tp'), may hold values from -0.125 to 0.125
- shared_gate: bfloat16 [2048, 512], replicated, may hold values from -0.125 to 0.125
- shared_up: bfloat16 [2048, 512], replicated, may hold values from -0.125 to 0.125
- shared_down: bfloat16 [512, 2048], replicated, may hold values from -0.25 to 0.25
Outputs:
- mixer_out: bfloat16 [3072, 2048], P(('ep', 'tp'))
- expert_out: bfloat16 [4096, 2048], P(('ep', 'tp'))
Inputs may be any that keep to these rules, and one draw needn't show every extreme that they name: `route_ids`: each row names 2 different experts. Within the rows of one device no expert is named more than 32 times, and in every draw some expert is named exactly 32 times within the rows of some device.
All inputs are finite; a program needn't handle non-finite values.
Results may differ from a plain program's by a relative error of at most 0.012.
Values may be sent and summed in bfloat16 or wider, within the bound.
A program may use at most 192 MiB of HBM per device.

v0:
```python
import jax
import jax.numpy as jnp
from jax import lax
from jax.sharding import PartitionSpec as P

DH = 64
TOPK = 2
SEQS = 1


norm_eps = 1e-06


def rms_scale(values, gain):
    values = values.astype(jnp.float32)
    scale = lax.rsqrt(jnp.mean(values * values, axis=-1, keepdims=True) + norm_eps)
    return (values * scale * gain.astype(jnp.float32)).astype(jnp.bfloat16)


def break_terms(queries, key_block, bias_block, query_start, key_start):
    row_count = queries.shape[0]
    heads_local = queries.shape[1] * queries.shape[2]
    key_count = key_block.shape[0]
    scores = jnp.einsum("rkgd,skd->kgrs", queries, key_block, preferred_element_type=jnp.float32)
    scores = scores.reshape(heads_local, row_count, key_count) * DH ** (-0.5)
    scores = scores + bias_block.astype(jnp.float32).T[:, None, :]
    query_pos = query_start + jnp.arange(row_count, dtype=jnp.int32)
    key_pos = key_start + jnp.arange(key_count, dtype=jnp.int32)
    visible = key_pos[None, :] < query_pos[:, None]
    keep = jnp.where(visible, -jax.nn.softplus(scores), 0.0)
    beyond = lax.cumsum(keep, axis=2, reverse=True) - keep
    return (scores, visible, keep, beyond)


def block_values(scores, visible, beyond, value_block, groups):
    heads_local, row_count, key_count = scores.shape
    kv_local = value_block.shape[1]
    weights = jnp.where(visible, jnp.exp(jax.nn.log_sigmoid(scores) + beyond), 0.0).astype(
        jnp.bfloat16
    )
    weights = weights.reshape(kv_local, groups, row_count, key_count)
    summed = jnp.einsum("kgrs,skd->kgrd", weights, value_block, preferred_element_type=jnp.float32)
    return summed.reshape(heads_local, row_count, DH)


def on_device(
    query_rows,
    key_rows,
    value_rows,
    break_bias,
    mixer_weight,
    mixer_gain,
    expert_input,
    expert_gain,
    route_ids,
    route_weights,
    expert_gate,
    expert_up,
    expert_down,
    shared_gate,
    shared_up,
    shared_down,
):
    row_count = query_rows.shape[0]
    heads_local = query_rows.shape[1] // DH
    kv_local = key_rows.shape[1] // DH
    groups = heads_local // kv_local
    queries = query_rows.reshape(row_count, kv_local, groups, DH)
    ep_size = lax.axis_size("ep")
    device = lax.axis_index("ep")
    query_start = device * row_count
    span_shards = ep_size // SEQS

    def wanted(shard):
        return (shard <= device) & (shard // span_shards == device // span_shards)

    def shard_slice(piece, index):
        return lax.dynamic_slice_in_dim(piece, index * row_count, row_count, 0)

    empty_totals = jnp.zeros((ep_size, heads_local, row_count), jnp.float32)
    empty_output = jnp.zeros((heads_local, row_count, DH), jnp.float32)
    empty_parts = jnp.zeros((ep_size, heads_local, row_count, DH), jnp.float32)
    key_piece = lax.all_gather(key_rows, "ep", axis=0, tiled=True)
    value_piece = lax.all_gather(value_rows, "ep", axis=0, tiled=True)
    bias_piece = lax.all_gather(break_bias, "ep", axis=0, tiled=True)

    def one_shard(index, current):
        parts, totals = current
        shard = index
        key_block = shard_slice(key_piece, index).reshape(row_count, kv_local, DH)
        value_block = shard_slice(value_piece, index).reshape(row_count, kv_local, DH)
        bias_block = shard_slice(bias_piece, index)

        def compute(unused):
            scores, visible, keep, beyond = break_terms(
                queries, key_block, bias_block, query_start, shard * row_count
            )
            return (
                block_values(scores, visible, beyond, value_block, groups),
                jnp.sum(keep, axis=2),
            )

        def skipped(unused):
            return (empty_output, jnp.zeros((heads_local, row_count), jnp.float32))

        block_part, total = lax.cond(wanted(shard), compute, skipped, None)
        parts = lax.dynamic_update_index_in_dim(parts, block_part, shard, 0)
        totals = lax.dynamic_update_index_in_dim(totals, total, shard, 0)
        return (parts, totals)

    parts, totals = lax.fori_loop(
        0, key_piece.shape[0] // row_count, one_shard, (empty_parts, empty_totals)
    )
    later = jnp.sum(totals, axis=0) - jnp.cumsum(totals, axis=0)
    output = jnp.sum(jnp.exp(later)[..., None] * parts, axis=0)
    attended = output.transpose(1, 0, 2).reshape(row_count, heads_local * DH).astype(jnp.bfloat16)
    block = attended
    projected = lax.psum_scatter(
        jnp.dot(block, mixer_weight, preferred_element_type=jnp.float32).astype(jnp.bfloat16),
        "tp",
        scatter_dimension=0,
        tiled=True,
    ).astype(jnp.float32)
    mixer_out = rms_scale(projected, mixer_gain)
    token_count = expert_input.shape[0]
    width = expert_input.shape[1]
    local_experts = expert_gate.shape[0]
    experts_all = local_experts * ep_size
    capacity = 2 * token_count * TOPK // experts_all
    tp_index = lax.axis_index("tp")
    normed = rms_scale(expert_input, expert_gain)
    flat = lax.dynamic_slice_in_dim(route_ids, tp_index * token_count, token_count, 0).reshape(-1)
    onehot = (flat[:, None] == jnp.arange(experts_all, dtype=jnp.int32)[None, :]).astype(jnp.int32)
    before = jnp.cumsum(onehot, axis=0) - onehot
    own_slots = flat * capacity + jnp.sum(before * onehot, axis=1)
    owners = jnp.full((experts_all * capacity,), token_count, jnp.int32)
    owners = owners.at[own_slots].set(jnp.arange(own_slots.shape[0], dtype=jnp.int32) // TOPK)
    padded = jnp.concatenate([normed, jnp.zeros((1, width), normed.dtype)], axis=0)
    outgoing = padded[owners].reshape(ep_size, local_experts, capacity, width)[None]
    arrived = lax.all_to_all(outgoing, "ep", split_axis=1, concat_axis=1, tiled=True)
    piece = lax.all_gather(arrived, "tp", axis=0, tiled=True)
    gate_proj = jnp.einsum(
        "pnecd,edf->pnecf", piece, expert_gate, preferred_element_type=jnp.float32
    )
    up_proj = jnp.einsum("pnecd,edf->pnecf", piece, expert_up, preferred_element_type=jnp.float32)
    hidden = (jax.nn.silu(gate_proj) * up_proj).astype(jnp.bfloat16)
    block = hidden
    summed = lax.psum_scatter(
        jnp.einsum(
            "pnecf,efd->pnecd", block, expert_down, preferred_element_type=jnp.float32
        ).astype(jnp.bfloat16),
        "tp",
        scatter_dimension=0,
        tiled=True,
    )
    returned = lax.all_to_all(
        summed.reshape(ep_size, local_experts * capacity, width),
        "ep",
        split_axis=0,
        concat_axis=0,
        tiled=True,
    )
    results = returned.reshape(experts_all * capacity, width)
    picked = results[own_slots].reshape(token_count, TOPK, width).astype(jnp.float32)
    routed = jnp.einsum("tk,tkd->td", route_weights, picked)
    shared_hidden = (
        jax.nn.silu(jnp.dot(normed, shared_gate, preferred_element_type=jnp.float32))
        * jnp.dot(normed, shared_up, preferred_element_type=jnp.float32)
    ).astype(jnp.bfloat16)
    expert_out = (
        routed + jnp.dot(shared_hidden, shared_down, preferred_element_type=jnp.float32)
    ).astype(jnp.bfloat16)
    return (mixer_out, expert_out)


def solution(mesh):
    return jax.shard_map(
        on_device,
        mesh=mesh,
        in_specs=(
            P("ep", "tp"),
            P("ep", "tp"),
            P("ep", "tp"),
            P("ep", "tp"),
            P("tp", None),
            P(),
            P(("ep", "tp"), None),
            P(),
            P("ep", None),
            P(("ep", "tp"), None),
            P("ep", None, "tp"),
            P("ep", None, "tp"),
            P("ep", "tp", None),
            P(),
            P(),
            P(),
        ),
        out_specs=(P(("ep", "tp"), None), P(("ep", "tp"), None)),
        check_vma=False,
    )
```

profile of v0, /device:TPU:0, one launch (start us, length us, event | category | flops | bytes accessed | tf_op | source)
XLA Modules:
  0.0 609.5 jit_solution(3167960819655452069)
XLA Ops:
  14.3 3.3 gather_fusion
  17.7 55.5 %all_to_all.10 = bf16[1,8,2,32,2048]{4,3,0,2,1:T(8,128)(2,1)S(1)} all-to-all(bf16[1,8,2,32,2048]{4,3,0,2,1:T(8,128)(2,1)} %bitcast.134), channel_id=1, replica_groups=mesh['ep'=8,'tp'=4] {'ep'}, dimensions={1} | all-to-all | bytes 4194304 | tf_op jit(solution)/shard_map/all_to_all | solution.py:140
  74.8 57.4 %all-gather.2.cloned.1.call-done = bf16[4,8,2,32,2048]{4,3,1,0,2:T(8,128)(2,1)} async-done(((bf16[1,8,2,32,2048]{4,3,1,0,2:T(8,128)(2,1)}), bf16[4,8,2,32,2048]{4,3,1,0,2:T(8,128)(2,1)}) %all-gather.2.cloned.1.call-update) | async-done | bytes 8388624 | tf_op jit(solution)/shard_map/all_gather | solution.py:141
  132.1 11.0 %fusion.26 = f32[2,4,8,32,512]{4,3,2,1,0:T(8,128)} fusion(bf16[4,8,2,32,2048]{4,3,1,0,2:T(8,128)(2,1)} %all-gather.2.cloned.1.call-done, bf16[2,2048,512]{2,1,0:T(8,128)(2,1)} %param.31), kind=kOutput, calls=%fused_computation.47 | convolution fusion | flops 4294967296 | bytes 16777216 | tf_op jit(solution)/shard_map/pnecd,edf->pnecf/dot_general | solution.py:145
  143.1 15.4 %convert_bitcast_fusion.2 = bf16[4,8,2,32,2048]{4,3,1,0,2:T(8,128)(2,1)} fusion(bf16[2,512,2048]{2,1,0:T(8,128)(2,1)} %param.32, f32[2,4,8,32,512]{4,3,2,1,0:T(8,128)} %fusion.26, bf16[4,8,2,32,2048]{4,3,1,0,2:T(8,128)(2,1)} %all-gather.2.cloned.1.call-done, bf16[2,2048,512]{2,1,0:T(8,128)(2,1)} %param.30), kind=kOutput, calls=%fused_computation.45 | convolution fusion | flops 8600420352 | bytes 29360128 | tf_op jit(solution)/shard_map/pnecf,efd->pnecd/dot_general | solution.py:149
  159.9 32.1 %all_gather.13 = bf16[3072,4]{0,1:T(4,128)(2,1)} all-gather(bf16[384,4]{0,1:T(4,128)(2,1)S(1)} %copy-done.8), channel_id=1, replica_groups=mesh['ep'=8,'tp'=4] {'ep'}, dimensions={0}, use_global_device_ids=true | all-gather | bytes 27648 | tf_op jit(solution)/shard_map/all_gather | solution.py:85
  192.0 34.8 %all_gather.12 = bf16[3072,128]{0,1:T(8,128)(2,1)} all-gather(bf16[384,128]{0,1:T(8,128)(2,1)S(1)} %copy.42), channel_id=1, replica_groups=mesh['ep'=8,'tp'=4] {'ep'}, dimensions={0}, use_global_device_ids=true | all-gather | bytes 884736 | tf_op jit(solution)/shard_map/all_gather | solution.py:83
  226.8 34.0 %all_gather.14 = bf16[3072,128]{0,1:T(8,128)(2,1)} all-gather(bf16[384,128]{0,1:T(8,128)(2,1)S(1)} %copy.44), channel_id=1, replica_groups=mesh['ep'=8,'tp'=4] {'ep'}, dimensions={0}, use_global_device_ids=true | all-gather | bytes 884736 | tf_op jit(solution)/shard_map/all_gather | solution.py:84
  260.9 41.2 %while.18 = (s32[]{:T(128)}, f32[8,4,384,64]{2,3,1,0:T(8,128)}, f32[8,4,384]{2,1,0:T(4,128)S(1)}, s32[]{:T(128)}, s32[]{:T(128)}, /*index=5*/s32[]{:T(128)}, bf1...) while((s32[]{:T(128)}, f32[8,4,384,64]{2,3,1,0:T(8,128)}, ...), condition=%wide.region_6.7_spmd, body=%wide.region_0.6_spmd.sunk | while | flops 250984336 | bytes 43047352 | solution.py:111
  260.9 34.5 %conditional.2 = (f32[1,4,384,64]{2,3,1,0:T(8,128)S(1)}, f32[1,4,384]{2,1,0:T(4,128)S(1)}) conditional(s32[]{:T(128)} %convert_element_type.126, () %tuple.76, (s32[]{:T(128)}, s32[]{:T(128)}, bf16[3072,128]{0,1:T(8,128)(2,1)}, bf16[384,2,2,64]{0,3,2,1:T(8,128)(2,1)S(1)}, bf16[3072,4]{0,1:T(4,128)(2,1)}, /*index=5*/bf16[3072,128]{0,1:T(8,128)(2,1)}) %tuple.77), branch_computations={%region_1.1_spmd, %region_2.5_spmd} | conditional | flops 250984320 | bytes 42247824 | solution.py:106
  262.7 3.4 fusion.17
  266.5 19.3 %fusion.2 = f32[4,384,3,128]{1,2,3,0:T(4,128)S(1)} fusion(f32[4,384,3,128]{1,3,2,0:T(8,128)} %bitcast.131, f32[4,3,128]{1,2,0:T(8,128)S(1)} %copy.38, pred[384,3,128]{0,1,2:T(4,128)(4,1)S(1)} %broadcast_compare_fusion), kind=kOutput, calls=%fused_computation.8 | output fusion | flops 80216064 | bytes 4872192 | tf_op jit(solution)/shard_map/reduce-window.10
  287.6 2.5 broadcast_add_fusion
  291.8 3.6 fusion.21
  302.1 2.3 multiply_reduce_fusion
  306.8 4.8 all-reduce.4.cloned.1.call-done
  311.6 2.4 constant_dynamic-slice_fusion.2
  315.4 241.3 %all-to-all-start.1 = ((bf16[8,64,2048]{2,1,0:T(8,128)(2,1)}), bf16[8,64,2048]{2,1,0:T(8,128)(2,1)}, u32[]{:S(2)}, u32[]{:S(2)}) async-start(bf16[8,64,2048]{2,1,0:T(8,128)(2,1)} %bitcast.135), calls=%async_computation.2 | async-start | bytes 4194304 | tf_op jit(solution)/shard_map/all_to_all | solution.py:156
  558.9 15.9 %reduce-scatter.5.cloned.1.call-done = bf16[96,2048]{1,0:T(8,128)(2,1)} async-done(((bf16[384,2048]{1,0:T(8,128)(2,1)}), bf16[96,2048]{1,0:T(8,128)(2,1)}) %reduce-scatter.5.cloned.1.call-update) | async-done | bytes 393232 | tf_op jit(solution)/shard_map/reduce_scatter | solution.py:118
  577.9 10.2 %all-to-all-done.1 = bf16[8,64,2048]{2,1,0:T(8,128)(2,1)} async-done(((bf16[8,64,2048]{2,1,0:T(8,128)(2,1)}), bf16[8,64,2048]{2,1,0:T(8,128)(2,1)}, u32[]{:S(2)}, u32[]{:S(2)}) %all-to-all-start.1) | async-done | bytes 2097184 | tf_op jit(solution)/shard_map/all_to_all | solution.py:156
  588.0 5.2 gather_fusion.1
  593.2 2.5 reshape.199
  595.8 3.5 fusion.61
  599.3 3.7 fusion.36
  (118 shorter events, 31.5 us)
Async XLA Ops:
  7.2 592.1 %copy-start = (bf16[512,2048]{1,0:T(8,128)(2,1)S(1)}, bf16[512,2048]{1,0:T(8,128)(2,1)}, u32[]{:S(2)}) copy-start(bf16[512,2048]{1,0:T(8,128)(2,1)} %param.35) | copy-start | bytes 6291460
  7.2 124.9 %all-gather.2.cloned.1.call-start = ((), (), s32[]{:S(2)}) async-start(), calls=%async_computation.4 | async-start | bytes 10485760 | tf_op jit(solution)/shard_map/all_gather | solution.py:141
  74.7 236.9 %all-reduce.4.cloned.1.call-start = ((), (), s32[]{:S(2)}) async-start(), calls=%async_computation.5 | async-start | bytes 16777216
  158.5 0.9 copy-start.5
  158.5 1.0 copy-start.6
  158.5 1.2 copy-start.4
  158.5 1.3 copy-start.8
  158.6 416.2 %reduce-scatter.5.cloned.1.call-start = ((), (), s32[]{:S(2)}) async-start(), calls=%async_computation.3 | async-start | bytes 1966080 | tf_op jit(solution)/shard_map/reduce_scatter | solution.py:118
  285.8 1.7 copy-start.1
  290.1 1.7 copy-start.2
  302.1 2.3 copy-start.3
  304.4 1.8 copy-start.10
  315.4 241.3 %copy-start.9 = (f32[128,2]{0,1:T(2,128)S(1)}, f32[128,2]{0,1:T(2,128)}, u32[]{:S(2)}) copy-start(f32[128,2]{0,1:T(2,128)} %param.29) | copy-start | bytes 3076
  315.4 241.4 %copy-start.7 = (bf16[2048]{0:T(1024)(128)(2,1)S(1)}, bf16[2048]{0:T(1024)(128)(2,1)}, u32[]{:S(2)}) copy-start(bf16[2048]{0:T(1024)(128)(2,1)} %param.25) | copy-start | bytes 12292
  315.4 272.7 %all-to-all-start.1 = ((bf16[8,64,2048]{2,1,0:T(8,128)(2,1)}), bf16[8,64,2048]{2,1,0:T(8,128)(2,1)}, u32[]{:S(2)}, u32[]{:S(2)}) async-start(bf16[8,64,2048]{2,1,0:T(8,128)(2,1)} %bitcast.135), calls=%async_computation.2 | async-start | bytes 4194304 | tf_op jit(solution)/shard_map/all_to_all | solution.py:156
Sparse Core Ops, SparseCore 0:
  74.8 57.2 all-gather.1
  158.7 152.8 all-reduce.3
  314.1 260.6 reduce-scatter.4
where the time goes:
time: 611 us; the launch traced here: 609 us
  starting transfers between devices  241 us (39%)
  blocking collectives  157 us (26%)
  waiting for transfers between devices  88.2 us (14%)
  matrix products  44.3 us (7%)
  other arithmetic  33 us (5%)
  local copies, waits for them, and re-layouts  31.7 us (5%)
  between operations  14 us (2%)
    all_to_all x1, starting transfers between devices, on_device(): lax.all_to_all(summed.reshape(ep_size, local_experts * capacity, width),...  241 us
    all_gather x1, waiting for transfers between devices, on_device(): piece = lax.all_gather(arrived, 'tp', axis=0, tiled=True)  57.4 us
    all_to_all x1, blocking collectives, on_device(): lax.all_to_all(outgoing, 'ep', split_axis=1, concat_axis=1, tiled=True)  55.5 us
    all_gather x1, blocking collectives, on_device(): key_piece = lax.all_gather(key_rows, 'ep', axis=0, tiled=True)  34.8 us
    all_gather x1, blocking collectives, on_device(): value_piece = lax.all_gather(value_rows, 'ep', axis=0, tiled=True)  34 us
    all_gather x1, blocking collectives, on_device(): bias_piece = lax.all_gather(break_bias, 'ep', axis=0, tiled=True)  32.1 us
    another operation x4, other arithmetic  20 us
    reduce_scatter x1, waiting for transfers between devices, on_device(): lax.psum_scatter(jnp.dot(block, mixer_weight, preferred_element_type=jnp....  15.9 us
  transfers between devices with their start and end apart: 4, of which 4 were waited for; matrix products, arithmetic and copies ran while one was open for 9% of the time, Pallas kernels for 0%

commit v1 on v0

v1 whole, which is shorter than its diff:
```python
import functools

import jax
import jax.numpy as jnp
from jax import lax
from jax.experimental import pallas as pl
from jax.experimental.pallas import tpu as pltpu
from jax.sharding import PartitionSpec as P


DH = 64
TOPK = 2
SEQS = 1


norm_eps = 1e-06


def rms_scale(values, gain):
    values = values.astype(jnp.float32)
    scale = lax.rsqrt(jnp.mean(values * values, axis=-1, keepdims=True) + norm_eps)
    return (values * scale * gain.astype(jnp.float32)).astype(jnp.bfloat16)


def attention_kernel(span_shards, place_ref, query_ref, key_ref, value_ref, bias_ref, out_ref):
    rows = query_ref.shape[1]
    device = place_ref[0]
    first = (device // span_shards) * span_shards
    queries = query_ref[0]
    row_of = lax.broadcasted_iota(jnp.int32, (rows, rows), 0)
    column_of = lax.broadcasted_iota(jnp.int32, (rows, rows), 1)
    visible = column_of < row_of
    after = visible.astype(jnp.float32).astype(jnp.bfloat16)

    def visit(shard, diagonal):
        start = pl.multiple_of(shard * rows, rows)
        keys = key_ref[pl.ds(start, rows), :]
        values = value_ref[pl.ds(start, rows), :]
        scores = lax.dot_general(
            queries, keys, (((1,), (1,)), ((), ())), preferred_element_type=jnp.float32
        )
        scores = scores + bias_ref[0, pl.ds(shard, 1), :]
        soft = jnp.log(1.0 + jnp.exp(-jnp.abs(scores)))
        keep = -(jnp.maximum(scores, 0.0) + soft)
        if diagonal:
            keep = jnp.where(visible, keep, 0.0)
        high = keep.astype(jnp.bfloat16)
        low = (keep - high.astype(jnp.float32)).astype(jnp.bfloat16)
        beyond = jnp.dot(high, after, preferred_element_type=jnp.float32) + jnp.dot(
            low, after, preferred_element_type=jnp.float32
        )
        weights = jnp.exp(jnp.minimum(scores, 0.0) - soft + beyond)
        if diagonal:
            weights = jnp.where(visible, weights, 0.0)
        total = beyond[:, 0:1] + keep[:, 0:1]
        summed = jnp.dot(weights.astype(jnp.bfloat16), values, preferred_element_type=jnp.float32)
        return summed, total

    output, later = visit(device, True)

    def earlier(step, current):
        output, later = current
        summed, total = visit(device - 1 - step, False)
        return output + jnp.exp(later) * summed, later + total

    output, later = lax.fori_loop(0, device - first, earlier, (output, later))
    out_ref[0] = output.astype(jnp.bfloat16)


def attend(query_rows, gathered, kv_width, heads_local, kv_local, span_shards, ep_size):
    rows = query_rows.shape[0]
    groups = heads_local // kv_local
    tokens = gathered.shape[0]
    keys = gathered[:, :kv_width]
    values = gathered[:, kv_width : 2 * kv_width]
    biases = gathered[:, 2 * kv_width : 2 * kv_width + heads_local].astype(jnp.float32).T
    biases = biases.reshape(heads_local, tokens // rows, rows)
    queries = (query_rows * jnp.bfloat16(DH ** (-0.5))).reshape(rows, heads_local, DH)
    queries = queries.transpose(1, 0, 2)
    place = jnp.arange(kv_width, dtype=jnp.int32) // DH
    owned = place[None, :] == (jnp.arange(heads_local, dtype=jnp.int32) // groups)[:, None]
    padded = jnp.where(owned[:, None, :], jnp.tile(queries, (1, 1, kv_local)), 0)
    device = lax.axis_index("ep").astype(jnp.int32).reshape(1)
    blocks = (ep_size + 1) // 2 * heads_local
    output = pl.pallas_call(
        functools.partial(attention_kernel, span_shards),
        out_shape=jax.ShapeDtypeStruct((heads_local, rows, kv_width), jnp.bfloat16),
        grid=(heads_local,),
        in_specs=[
            pl.BlockSpec(memory_space=pltpu.SMEM),
            pl.BlockSpec((1, rows, kv_width), lambda h: (h, 0, 0)),
            pl.BlockSpec((tokens, kv_width), lambda h: (0, 0)),
            pl.BlockSpec((tokens, kv_width), lambda h: (0, 0)),
            pl.BlockSpec((1, tokens // rows, rows), lambda h: (h, 0, 0)),
        ],
        out_specs=pl.BlockSpec((1, rows, kv_width), lambda h: (h, 0, 0)),
        compiler_params=pltpu.CompilerParams(
            dimension_semantics=("arbitrary",), vmem_limit_bytes=32 * 1024 * 1024
        ),
        cost_estimate=pl.CostEstimate(
            flops=40 * 2 * blocks * rows * rows * rows,
            bytes_accessed=4 * tokens * kv_width,
            transcendentals=3 * blocks * rows * rows,
        ),
        name="attention",
    )(device, padded, keys, values, biases)
    picked = [
        output[head, :, (head // groups) * DH : (head // groups + 1) * DH]
        for head in range(heads_local)
    ]
    return jnp.concatenate(picked, axis=1)


def on_device(
    query_rows,
    key_rows,
    value_rows,
    break_bias,
    mixer_weight,
    mixer_gain,
    expert_input,
    expert_gain,
    route_ids,
    route_weights,
    expert_gate,
    expert_up,
    expert_down,
    shared_gate,
    shared_up,
    shared_down,
):
    heads_local = query_rows.shape[1] // DH
    kv_width = key_rows.shape[1]
    kv_local = kv_width // DH
    ep_size = lax.axis_size("ep")
    span_shards = ep_size // SEQS
    bias_pad = (-heads_local) % 128
    own_terms = jnp.concatenate(
        [key_rows, value_rows, jnp.pad(break_bias, ((0, 0), (0, bias_pad)))], axis=1
    )
    gathered = lax.all_gather(own_terms, "ep", axis=0, tiled=True)

    token_count = expert_input.shape[0]
    local_experts = expert_gate.shape[0]
    experts_all = local_experts * ep_size
    capacity = 2 * token_count * TOPK // experts_all
    slots = ep_size * capacity
    tp_index = lax.axis_index("tp")
    normed = rms_scale(expert_input, expert_gain)
    ids = lax.dynamic_slice_in_dim(route_ids, tp_index * token_count, token_count, 0)
    flat = ids.reshape(-1)
    onehot = (flat[:, None] == jnp.arange(experts_all, dtype=jnp.int32)[None, :]).astype(jnp.int32)
    before = jnp.cumsum(onehot, axis=0) - onehot
    rank = jnp.sum(before * onehot, axis=1).reshape(token_count, TOPK)
    position = (ids // local_experts) * capacity + rank
    slot_range = jnp.arange(slots, dtype=jnp.int32)
    arrived, mixing = [], []
    for expert in range(local_experts):
        slot_of = jnp.where(ids % local_experts == expert, position, -1)
        named = slot_of[:, :, None] == slot_range[None, None, :]
        chosen = jnp.any(named, axis=1).astype(jnp.bfloat16)
        weight = jnp.sum(jnp.where(named, route_weights[:, :, None], 0.0), axis=1)
        high = weight.astype(jnp.bfloat16)
        low = (weight - high.astype(jnp.float32)).astype(jnp.bfloat16)
        mixing.append((high, low))
        outgoing = lax.dot_general(
            chosen, normed, (((0,), (0,)), ((), ())), preferred_element_type=jnp.float32
        ).astype(jnp.bfloat16)
        arrived.append(lax.all_to_all(outgoing, "ep", split_axis=0, concat_axis=0, tiled=True))
    pieces = [lax.all_gather(rows, "tp", axis=0, tiled=True) for rows in arrived]

    attended = attend(
        query_rows, gathered, kv_width, heads_local, kv_local, span_shards, ep_size
    )
    shared_hidden = (
        jax.nn.silu(jnp.dot(normed, shared_gate, preferred_element_type=jnp.float32))
        * jnp.dot(normed, shared_up, preferred_element_type=jnp.float32)
    ).astype(jnp.bfloat16)
    expert_out = jnp.dot(shared_hidden, shared_down, preferred_element_type=jnp.float32)
    expert_out = lax.optimization_barrier(expert_out)

    returned = []
    for expert in range(local_experts):
        piece = pieces[expert]
        gate_proj = jnp.dot(piece, expert_gate[expert], preferred_element_type=jnp.float32)
        up_proj = jnp.dot(piece, expert_up[expert], preferred_element_type=jnp.float32)
        hidden = (jax.nn.silu(gate_proj) * up_proj).astype(jnp.bfloat16)
        part = jnp.dot(hidden, expert_down[expert], preferred_element_type=jnp.float32)
        summed = lax.psum_scatter(
            part.astype(jnp.bfloat16), "tp", scatter_dimension=0, tiled=True
        )
        returned.append(lax.all_to_all(summed, "ep", split_axis=0, concat_axis=0, tiled=True))
    projected = lax.psum_scatter(
        jnp.dot(attended, mixer_weight, preferred_element_type=jnp.float32).astype(jnp.bfloat16),
        "tp",
        scatter_dimension=0,
        tiled=True,
    ).astype(jnp.float32)
    mixer_out = rms_scale(projected, mixer_gain)
    for (high, low), results in zip(mixing, returned):
        expert_out = (
            expert_out
            + jnp.dot(high, results, preferred_element_type=jnp.float32)
            + jnp.dot(low, results, preferred_element_type=jnp.float32)
        )
    return (mixer_out, expert_out.astype(jnp.bfloat16))


def solution(mesh):
    return jax.shard_map(
        on_device,
        mesh=mesh,
        in_specs=(
            P("ep", "tp"),
            P("ep", "tp"),
            P("ep", "tp"),
            P("ep", "tp"),
            P("tp", None),
            P(),
            P(("ep", "tp"), None),
            P(),
            P("ep", None),
            P(("ep", "tp"), None),
            P("ep", None, "tp"),
            P("ep", None, "tp"),
            P("ep", "tp", None),
            P(),
            P(),
            P(),
        ),
        out_specs=(P(("ep", "tp"), None), P(("ep", "tp"), None)),
        check_vma=False,
    )
```

time: 611 us -> 313 us (0.51)
  starting transfers between devices: 241 us -> 11.4 us
  blocking collectives: 157 us -> 61.9 us
  waiting for transfers between devices: 88.2 us -> 151 us
  local copies, waits for them, and re-layouts: 31.7 us -> 6.48 us
  other arithmetic: 33 us -> 9.54 us
  matrix products: 44.3 us -> 53.9 us
    all_to_all x1 -> x2, starting transfers between devices: 241 us -> 11 us  [on_device(): lax.all_to_all(summed, 'ep', split_axis=0, concat_axis=0, tiled=True)]
    all_gather x3 -> x0, blocking collectives: 101 us -> none  [the longest x1 34.8 us: on_device(): key_piece = lax.all_gather(key_rows, 'ep', axis=0, tiled=True)]
    reduce_scatter x1 -> x3, waiting for transfers between devices: 15.9 us -> 94.5 us  [the longest x2 73.3 us: on_device(): lax.psum_scatter(part.astype(jnp.bfloat16), 'tp', scatter_dimension=0, ti...]
    another operation x6 -> x2, other arithmetic: 22.4 us -> 0.63 us
    all_to_all x1 -> x2, waiting for transfers between devices: 10.2 us -> 0.01 us  [on_device(): lax.all_to_all(summed, 'ep', split_axis=0, concat_axis=0, tiled=True)]
    dot_general x6 -> x11, matrix products: 38.6 us -> 48.3 us  [the longest x2 22.7 us: on_device(): jnp.dot(hidden, expert_down[expert], preferred_element_type=jnp.float32)]
    gather x2 -> x0, local copies, waits for them, and re-layouts: 8.55 us -> none  [the longest x1 5.21 us: on_device(): results[own_slots].reshape(token_count, TOPK, width).astype(jnp.float32)]
    all_to_all x1 -> x2, blocking collectives: 55.5 us -> 61.9 us  [on_device(): lax.all_to_all(outgoing, 'ep', split_axis=0, concat_axis=0, tiled=True)]
  transfers between devices with their start and end apart: 4 -> 8, of which waited for: 4 -> 6; matrix products, arithmetic and copies ran while one was open for 9% -> 19% of each run, Pallas kernels for 0% -> 1%
where the time goes in v1:
time: 313 us; the launch traced here: 312 us
  waiting for transfers between devices  151 us (48%)
  blocking collectives  61.9 us (20%)
  matrix products  53.9 us (17%)
  between operations  14.4 us (5%)
  starting transfers between devices  11.4 us (4%)
  other arithmetic  9.54 us (3%)
  local copies, waits for them, and re-layouts  6.48 us (2%)
  Pallas kernels  3.87 us (1%)
    reduce_scatter x2, waiting for transfers between devices, on_device(): lax.psum_scatter(part.astype(jnp.bfloat16), 'tp', scatter_dimension=0, ti...  73.3 us
    all_to_all x2, blocking collectives, on_device(): lax.all_to_all(outgoing, 'ep', split_axis=0, concat_axis=0, tiled=True)  61.9 us
    all_gather x1, waiting for transfers between devices, on_device(): gathered = lax.all_gather(own_terms, 'ep', axis=0, tiled=True)  37.3 us
    dot_general x2, matrix products, on_device(): jnp.dot(hidden, expert_down[expert], preferred_element_type=jnp.float32)  22.7 us
    reduce_scatter x1, waiting for transfers between devices, on_device(): lax.psum_scatter(jnp.dot(attended, mixer_weight, preferred_element_type=j...  21.2 us
    all_gather x2, waiting for transfers between devices, on_device(): lax.all_gather(rows, 'tp', axis=0, tiled=True)  18.8 us
    dot_general x2, matrix products, on_device(): jnp.dot(piece, expert_up[expert], preferred_element_type=jnp.float32)  13 us
    all_to_all x2, starting transfers between devices, on_device(): lax.all_to_all(summed, 'ep', split_axis=0, concat_axis=0, tiled=True)  11 us
  transfers between devices with their start and end apart: 8, of which 6 were waited for; matrix products, arithmetic and copies ran while one was open for 19% of the time, Pallas kernels for 1%

profile of v1, /device:TPU:0, one launch (start us, length us, event | category | flops | bytes accessed | tf_op | source)
XLA Modules:
  0.0 312.2 jit_solution(8453555600302776647)
XLA Ops:
  13.4 33.0 %all_to_all.48 = bf16[8,32,2048]{2,1,0:T(8,128)(2,1)} all-to-all(bf16[8,32,2048]{2,1,0:T(8,128)(2,1)S(1)} %bitcast.86), channel_id=1, replica_groups=mesh['ep'=8,'tp'=4] {'ep'}, dimensions={0} | all-to-all | bytes 2097152 | tf_op jit(solution)/shard_map/all_to_all | solution.py:169
  47.2 29.0 %all_to_all.49 = bf16[8,32,2048]{2,1,0:T(8,128)(2,1)} all-to-all(bf16[8,32,2048]{2,1,0:T(8,128)(2,1)S(1)} %bitcast.87), channel_id=1, replica_groups=mesh['ep'=8,'tp'=4] {'ep'}, dimensions={0} | all-to-all | bytes 2097152 | tf_op jit(solution)/shard_map/all_to_all | solution.py:169
  77.3 2.7 all-gather.6.cloned.1.call-done
  80.0 6.5 %fusion.7 = f32[1024,512]{1,0:T(8,128)} fusion(bf16[1024,2048]{1,0:T(8,128)(2,1)} %all-gather.6.cloned.1.call-done, bf16[2,2048,512]{2,1,0:T(8,128)(2,1)} %param.27), kind=kOutput, calls=%fused_computation.16 | convolution fusion | flops 2147483648 | bytes 8388608 | tf_op jit(solution)/shard_map/dot_general | solution.py:186
  86.5 11.9 %convolution_convert_fusion.1 = bf16[1024,2048]{1,0:T(8,128)(2,1)} fusion(bf16[2,512,2048]{2,1,0:T(8,128)(2,1)} %param.28, f32[1024,512]{1,0:T(8,128)} %fusion.7, bf16[1024,2048]{1,0:T(8,128)(2,1)} %all-gather.6.cloned.1.call-done, bf16[2,2048,512]{2,1,0:T(8,128)(2,1)} %param.26), kind=kOutput, calls=%fused_computation.1 | convolution fusion | flops 4300210176 | bytes 14680064 | tf_op jit(solution)/shard_map/dot_general | solution.py:188
  100.0 16.1 %all-gather.8.cloned.1.call-done = bf16[1024,2048]{1,0:T(8,128)(2,1)} async-done(((bf16[256,2048]{1,0:T(8,128)(2,1)}), bf16[1024,2048]{1,0:T(8,128)(2,1)}) %all-gather.8.cloned.1.call-update) | async-done | bytes 4194320 | tf_op jit(solution)/shard_map/all_gather | solution.py:170
  116.1 6.5 %fusion.2 = f32[1024,512]{1,0:T(8,128)} fusion(bf16[1024,2048]{1,0:T(8,128)(2,1)} %all-gather.8.cloned.1.call-done, bf16[2,2048,512]{2,1,0:T(8,128)(2,1)} %param.27), kind=kOutput, calls=%fused_computation.11 | convolution fusion | flops 2147483648 | bytes 8388608 | tf_op jit(solution)/shard_map/dot_general | solution.py:186
  122.5 10.8 %convolution_convert_fusion = bf16[1024,2048]{1,0:T(8,128)(2,1)} fusion(bf16[2,512,2048]{2,1,0:T(8,128)(2,1)} %param.28, f32[1024,512]{1,0:T(8,128)} %fusion.2, bf16[1024,2048]{1,0:T(8,128)(2,1)} %all-gather.8.cloned.1.call-done, bf16[2,2048,512]{2,1,0:T(8,128)(2,1)} %param.26), kind=kOutput, calls=%fused_computation | convolution fusion | flops 4300210176 | bytes 14680064 | tf_op jit(solution)/shard_map/dot_general | solution.py:188
  133.4 37.3 %all-gather.4.cloned.1.call-done = bf16[3072,384]{1,0:T(8,128)(2,1)} async-done(((bf16[384,384]{1,0:T(8,128)(2,1)}), bf16[3072,384]{1,0:T(8,128)(2,1)}) %all-gather.4.cloned.1.call-update) | async-done | bytes 2359312 | tf_op jit(solution)/shard_map/all_gather | solution.py:141
  170.7 2.4 slice_convert_fusion
  173.1 1.9 copy.39.bias_ref
  176.5 3.9 %attention.1 = bf16[4,384,128]{2,1,0:T(8,128)(2,1)S(1)} custom-call(s32[1]{0:T(128)} %bitcast.place_ref, bf16[4,384,128]{2,1,0:T(8,128)(2,1)S(1)} %broadcast_select_fusion.query_ref, bf16[3072,128]{1,0:T(8,128)(2,1)S(1)} %get-tuple-element.5.key_ref, bf16[3072,128]{1,0:T(8,128)(2,1)S(1)} %get-tuple-element.4.value_ref, f32[4,8,384]{2,1,0:T(8,128)S(1)} %copy.39.bias_ref), custom_call_target="tpu_custom_call" | custom-call | flops 72477573120 | bytes 1572864 | tf_op jit(solution)/shard_map/attention/pallas_call | solution.py:85
  182.3 33.9 %reduce-scatter.6.cloned.1.call-done = bf16[256,2048]{1,0:T(8,128)(2,1)} async-done(((bf16[1024,2048]{1,0:T(8,128)(2,1)}), bf16[256,2048]{1,0:T(8,128)(2,1)}) %reduce-scatter.6.cloned.1.call-update) | async-done | bytes 1048592 | tf_op jit(solution)/shard_map/reduce_scatter | solution.py:189
  216.2 5.5 %all-to-all-start.1 = ((bf16[8,32,2048]{2,1,0:T(8,128)(2,1)}), bf16[8,32,2048]{2,1,0:T(8,128)(2,1)}, u32[]{:S(2)}, u32[]{:S(2)}) async-start(bf16[8,32,2048]{2,1,0:T(8,128)(2,1)} %bitcast.89), calls=%async_computation.3 | async-start | bytes 2097152 | tf_op jit(solution)/shard_map/all_to_all | solution.py:192
  221.7 2.1 fusion.70
  223.8 39.4 %reduce-scatter.8.cloned.1.call-done = bf16[256,2048]{1,0:T(8,128)(2,1)} async-done(((bf16[1024,2048]{1,0:T(8,128)(2,1)}), bf16[256,2048]{1,0:T(8,128)(2,1)}) %reduce-scatter.8.cloned.1.call-update) | async-done | bytes 1048592 | tf_op jit(solution)/shard_map/reduce_scatter | solution.py:189
  263.2 5.5 %all-to-all-start.3 = ((bf16[8,32,2048]{2,1,0:T(8,128)(2,1)}), bf16[8,32,2048]{2,1,0:T(8,128)(2,1)}, u32[]{:S(2)}, u32[]{:S(2)}) async-start(bf16[8,32,2048]{2,1,0:T(8,128)(2,1)} %bitcast.90), calls=%async_computation.6 | async-start | bytes 2097152 | tf_op jit(solution)/shard_map/all_to_all | solution.py:192
  268.7 3.5 %fusion.22 = f32[128,2048]{1,0:T(8,128)} fusion(bf16[512,2048]{1,0:T(8,128)(2,1)S(1)} %copy-done, bf16[2048,512]{1,0:T(8,128)(2,1)} %param.30, f32[128,512]{1,0:T(8,128)S(1)} %fusion.70, bf16[128,2048]{1,0:T(8,128)(2,1)S(1)} %copy-done.1, f32[2048]{0:T(1024)S(1)} %convert_element_type.82, f32[128]{0:T(128)S(1)} %add_rsqrt_fusion), kind=kOutput, calls=%fused_computation.32 | convolution fusion | flops 538312704 | bytes 6038016 | tf_op jit(solution)/shard_map/dot_general | solution.py:179
  272.4 21.2 %reduce-scatter.4.cloned.1.call-done = bf16[96,2048]{1,0:T(8,128)(2,1)} async-done(((bf16[384,2048]{1,0:T(8,128)(2,1)}), bf16[96,2048]{1,0:T(8,128)(2,1)}) %reduce-scatter.4.cloned.1.call-update) | async-done | bytes 393232 | tf_op jit(solution)/shard_map/reduce_scatter | solution.py:193
  294.8 1.9 fusion.32
  296.7 1.8 convolution_add_fusion.3
  298.6 2.6 convolution_add_fusion.2
  301.2 1.8 convolution_add_fusion.1
  303.0 2.3 fusion
  (70 shorter events, 14.4 us)
Async XLA Ops:
  7.2 261.5 %copy-start = (bf16[512,2048]{1,0:T(8,128)(2,1)S(1)}, bf16[512,2048]{1,0:T(8,128)(2,1)}, u32[]{:S(2)}) copy-start(bf16[512,2048]{1,0:T(8,128)(2,1)} %param.31) | copy-start | bytes 6291460
  7.2 72.8 %all-gather.6.cloned.1.call-start = ((), (), s32[]{:S(2)}) async-start(), calls=%async_computation.9 | async-start | bytes 5242880 | tf_op jit(solution)/shard_map/all_gather | solution.py:170
  11.7 34.9 %copy-start.1 = (bf16[128,2048]{1,0:T(8,128)(2,1)S(1)}, bf16[128,2048]{1,0:T(8,128)(2,1)}, u32[]{:S(2)}) copy-start(bf16[128,2048]{1,0:T(8,128)(2,1)} %param.22) | copy-start | bytes 1572868
  46.4 69.7 %all-gather.8.cloned.1.call-start = ((), (), s32[]{:S(2)}) async-start(), calls=%async_computation.11 | async-start | bytes 5242880 | tf_op jit(solution)/shard_map/all_gather | solution.py:170
  46.6 29.6 %copy-start.7 = (bf16[384,4]{0,1:T(4,128)(2,1)S(1)}, bf16[384,4]{0,1:T(4,128)(2,1)}, u32[]{:S(2)}) copy-start(bf16[384,4]{0,1:T(4,128)(2,1)} %param.19) | copy-start | bytes 9220
  46.7 29.8 %copy-start.4 = (bf16[384,128]{1,0:T(8,128)(2,1)S(1)}, bf16[384,128]{1,0:T(8,128)(2,1)}, u32[]{:S(2)}) copy-start(bf16[384,128]{1,0:T(8,128)(2,1)} %param.18) | copy-start | bytes 294916
  46.7 29.8 %copy-start.5 = (bf16[384,128]{1,0:T(8,128)(2,1)S(1)}, bf16[384,128]{1,0:T(8,128)(2,1)}, u32[]{:S(2)}) copy-start(bf16[384,128]{1,0:T(8,128)(2,1)} %param.17) | copy-start | bytes 294916
  76.2 94.5 %all-gather.4.cloned.1.call-start = ((), (), s32[]{:S(2)}) async-start(), calls=%async_computation.7 | async-start | bytes 2654208 | tf_op jit(solution)/shard_map/all_gather | solution.py:141
  77.2 139.0 %reduce-scatter.6.cloned.1.call-start = ((), (), s32[]{:S(2)}) async-start(), calls=%async_computation.10 | async-start | bytes 5242880 | tf_op jit(solution)/shard_map/reduce_scatter | solution.py:189
  98.4 0.9 copy-start.3
  98.4 164.7 %reduce-scatter.8.cloned.1.call-start = ((), (), s32[]{:S(2)}) async-start(), calls=%async_computation.12 | async-start | bytes 5242880 | tf_op jit(solution)/shard_map/reduce_scatter | solution.py:189
  133.3 160.3 %reduce-scatter.4.cloned.1.call-start = ((), (), s32[]{:S(2)}) async-start(), calls=%async_computation.8 | async-start | bytes 1966080 | tf_op jit(solution)/shard_map/reduce_scatter | solution.py:193
  176.4 4.0 %copy-start.2 = (bf16[256,2048]{1,0:T(8,128)(2,1)S(1)}, bf16[256,2048]{1,0:T(8,128)(2,1)}, u32[]{:S(2)}) copy-start(bf16[256,2048]{1,0:T(8,128)(2,1)} %param.20) | copy-start | bytes 3145732
  216.2 47.0 %all-to-all-start.1 = ((bf16[8,32,2048]{2,1,0:T(8,128)(2,1)}), bf16[8,32,2048]{2,1,0:T(8,128)(2,1)}, u32[]{:S(2)}, u32[]{:S(2)}) async-start(bf16[8,32,2048]{2,1,0:T(8,128)(2,1)} %bitcast.89), calls=%async_computation.3 | async-start | bytes 2097152 | tf_op jit(solution)/shard_map/all_to_all | solution.py:192
  263.2 38.0 %all-to-all-start.3 = ((bf16[8,32,2048]{2,1,0:T(8,128)(2,1)}), bf16[8,32,2048]{2,1,0:T(8,128)(2,1)}, u32[]{:S(2)}, u32[]{:S(2)}) async-start(bf16[8,32,2048]{2,1,0:T(8,128)(2,1)} %bitcast.90), calls=%async_computation.6 | async-start | bytes 2097152 | tf_op jit(solution)/shard_map/all_to_all | solution.py:192
  268.7 3.5 %copy-start.6 = (bf16[2048]{0:T(1024)(128)(2,1)S(1)}, bf16[2048]{0:T(1024)(128)(2,1)}, u32[]{:S(2)}) copy-start(bf16[2048]{0:T(1024)(128)(2,1)} %param.21) | copy-start | bytes 12292
  268.7 3.5 %copy-start.8 = (f32[128,2]{0,1:T(2,128)S(1)}, f32[128,2]{0,1:T(2,128)}, u32[]{:S(2)}) copy-start(f32[128,2]{0,1:T(2,128)} %param.25) | copy-start | bytes 3076
Sparse Core Ops, SparseCore 0:
  46.5 33.4 all-gather.5
  81.6 34.4 all-gather.7
  118.8 51.8 all-gather.3
  173.0 43.1 reduce-scatter.5
  218.6 44.5 reduce-scatter.7
  265.6 28.0 reduce-scatter.3
